TPU v7x, 32 devices: a whole 2x2x4 slice. The times are simulated.
32 devices in a mesh: ep: 8 (over z, core), tp: 4 (over y, x).
Axes of the slice: x: 2, y: 2, z: 4, core: 2. Of those that a mesh axis runs over, the one named last changes fastest.
Arguments:
- q_latent: bfloat16 [1536, 512], P('ep'), may hold values from -6 to 6
- kv_latent: bfloat16 [1536, 256], P('ep'), may hold values from -6 to 6
- rope_key: bfloat16 [1536, 64], P('ep'), may hold values from -900 to 900
- q_gain: float32 [512], replicated, may hold values from 0.1 to 1.9
- kv_gain: float32 [256], replicated, may hold values from 0.1 to 1.9
- w_query: bfloat16 [512, 3072], P(None, 'tp'), may hold values from -0.25 to 0.25
- w_key: bfloat16 [256, 2048], P(None, 'tp'), may hold values from -0.375 to 0.375
- w_value: bfloat16 [256, 2048], P(None, 'tp'), may hold values from -0.375 to 0.375
- w_mix_out: bfloat16 [2048, 2048], P('tp'), may hold values from -0.125 to 0.125
- expert_in: bfloat16 [1024, 2048], P('ep'), may hold values from -6 to 6
- norm_gain: float32 [2048], replicated, may hold values from 0.1 to 1.9
- routes: int32 [1024, 2], P('ep'), may hold values from 0 to 7, all different within a row; in each aligned block of 128 rows (0 to 127, 128 to 255, ...) at most 64 rows name the same one
- route_scores: float32 [1024, 2], P('ep'), may hold values from 0.05 to 1
- w_gate: bfloat16 [8, 2048, 4096], P('ep', None, 'tp'), may hold values from -0.125 to 0.125
- w_up: bfloat16 [8, 2048, 4096], P('ep', None, 'tp'), may hold values from -0.125 to 0.125
- w_down: bfloat16 [8, 4096, 2048], P('ep', 'tp'), may hold values from -0.125 to 0.125
Outputs:
- mixed: bfloat16 [1536, 2048], P(('ep', 'tp'))
- expert_out: bfloat16 [1024, 2048], P('ep', 'tp')
Inputs may be any that keep to these rules, and one draw needn't show every extreme that they name: `routes`: each row names 2 different experts; in the rows of one index of ep no expert is named by more than 64 rows, a bound that some block reaches.
All inputs are finite; a program needn't handle non-finite values.
Results may differ from a plain program's by a relative error of at most 0.03.
The roundings to bfloat16 on the way count: a program that leaves them out, or rounds other values in their place, can miss the bound.
Values may be sent and summed in bfloat16 or wider, within the bound.
A program may use at most 64 MiB of HBM per device.

v0:
```python
import jax
import jax.numpy as jnp
from jax import lax
from jax.sharding import PartitionSpec as P

NOPE = 128
ROPE = 64
VDIM = 128


eps_norm = 1e-05
rope_base = 10000.0


def rms_scale(values, gain):
    wide = values.astype(jnp.float32)
    return wide * lax.rsqrt(jnp.mean(wide * wide, -1, keepdims=True) + eps_norm) * gain


def rotate(values, cosine, sine):
    first, second = jnp.split(values, 2, axis=-1)
    return jnp.concatenate([first * cosine - second * sine, first * sine + second * cosine], -1)


def angles(positions):
    inverse = rope_base ** (-jnp.arange(0, ROPE, 2).astype(jnp.float32) / ROPE)
    phase = positions[:, None] * inverse[None, :]
    return (jnp.cos(phase), jnp.sin(phase))


def mixer(q_latent, kv_latent, rope_key, q_gain, kv_gain, w_query, w_key, w_value, w_mix_out):
    token_count = q_latent.shape[0]
    head_count = w_key.shape[1] // NOPE
    offset = lax.axis_index("ep") * token_count
    positions = (offset + jnp.arange(token_count, dtype=jnp.int32)).astype(jnp.float32)
    cosine, sine = angles(positions)
    q_normed = rms_scale(q_latent, q_gain).astype(jnp.bfloat16)
    kv_normed = rms_scale(kv_latent, kv_gain).astype(jnp.bfloat16)
    key_turned = rotate(rope_key.astype(jnp.float32), cosine, sine).astype(jnp.bfloat16)
    query = jnp.dot(q_normed, w_query, preferred_element_type=jnp.float32).astype(jnp.bfloat16)
    query = query.reshape(token_count, head_count, NOPE + ROPE)
    q_pass = query[:, :, :NOPE]
    q_turned = rotate(
        query[:, :, NOPE:].astype(jnp.float32), cosine[:, None, :], sine[:, None, :]
    ).astype(jnp.bfloat16)
    factor = (NOPE + ROPE) ** (-0.5)
    peak = jnp.full((head_count, token_count), -jnp.inf, jnp.float32)
    total = jnp.zeros((head_count, token_count), jnp.float32)
    summed = jnp.zeros((token_count, head_count, VDIM), jnp.float32)
    latent = lax.all_gather(kv_normed, "ep", axis=0, tiled=True)
    turned = lax.all_gather(key_turned, "ep", axis=0, tiled=True)
    count = latent.shape[0]
    keys = jnp.dot(latent, w_key, preferred_element_type=jnp.float32).astype(jnp.bfloat16)
    keys = keys.reshape(count, head_count, NOPE)
    values = jnp.dot(latent, w_value, preferred_element_type=jnp.float32).astype(jnp.bfloat16)
    values = values.reshape(count, head_count, VDIM)
    scores = jnp.einsum("qhd,khd->hqk", q_pass, keys, preferred_element_type=jnp.float32)
    scores = (
        scores + jnp.einsum("qhd,kd->hqk", q_turned, turned, preferred_element_type=jnp.float32)
    ) * factor
    fresh = jnp.max(scores, -1)
    fade = jnp.exp(peak - fresh)
    weights = jnp.exp(scores - fresh[:, :, None])
    total = total * fade + jnp.sum(weights, -1)
    update = jnp.einsum(
        "hqk,khd->qhd", weights.astype(jnp.bfloat16), values, preferred_element_type=jnp.float32
    )
    summed = summed * jnp.transpose(fade)[:, :, None] + update
    peak, total, summed = (fresh, total, summed)
    attended = (summed / jnp.transpose(total)[:, :, None]).astype(jnp.bfloat16)
    attended = attended.reshape(token_count, head_count * VDIM)
    return lax.psum_scatter(
        jnp.dot(attended, w_mix_out, preferred_element_type=jnp.float32).astype(jnp.bfloat16),
        "tp",
        scatter_dimension=0,
        tiled=True,
    )


def experts(expert_in, norm_gain, routes, route_scores, w_gate, w_up, w_down):
    token_count, width = expert_in.shape
    choose = routes.shape[1]
    expert_count = lax.axis_size("ep")
    slots = 2 * choose * token_count // expert_count
    wide = expert_in.astype(jnp.float32)
    centered = wide - jnp.mean(wide, -1, keepdims=True)
    normed = (
        centered
        * lax.rsqrt(jnp.mean(centered * centered, -1, keepdims=True) + eps_norm)
        * norm_gain
    ).astype(jnp.bfloat16)
    shares = route_scores / jnp.sum(route_scores, -1, keepdims=True)
    flat_expert = routes.reshape(-1)
    onehot = (flat_expert[:, None] == jnp.arange(expert_count, dtype=jnp.int32)[None, :]).astype(
        jnp.int32
    )
    before = jnp.sum((jnp.cumsum(onehot, 0) - onehot) * onehot, 1)
    target = flat_expert * slots + before
    source = jnp.arange(token_count * choose, dtype=jnp.int32) // choose
    table = jnp.full((expert_count * slots,), token_count, jnp.int32).at[target].set(source)
    padded = jnp.concatenate([normed, jnp.zeros((1, width), jnp.bfloat16)], 0)
    outgoing = padded[table].reshape(expert_count, slots, width)
    gate_weight = w_gate[0]
    up_weight = w_up[0]
    down_weight = w_down[0]
    arrived = lax.all_to_all(outgoing, "ep", split_axis=0, concat_axis=0, tiled=True).reshape(
        expert_count * slots, width
    )
    gate = jnp.dot(arrived, gate_weight, preferred_element_type=jnp.float32)
    up = jnp.dot(arrived, up_weight, preferred_element_type=jnp.float32)
    hidden = (jax.nn.silu(gate) * up).astype(jnp.bfloat16)
    summed = lax.psum_scatter(
        lax.dot_general(
            down_weight, hidden, (((0,), (1,)), ((), ())), preferred_element_type=jnp.float32
        ).astype(jnp.bfloat16),
        "tp",
        scatter_dimension=0,
        tiled=True,
    )
    feature_count = summed.shape[0]
    returned = lax.all_to_all(
        summed.reshape(feature_count, expert_count, slots),
        "ep",
        split_axis=1,
        concat_axis=1,
        tiled=True,
    )
    picked = jnp.take(returned.reshape(feature_count, expert_count * slots), target, axis=1)
    picked = picked.reshape(feature_count, token_count, choose).astype(jnp.float32)
    combined = jnp.sum(picked * shares[None, :, :], -1)
    return jnp.transpose(combined).astype(jnp.bfloat16)


def body(
    q_latent,
    kv_latent,
    rope_key,
    q_gain,
    kv_gain,
    w_query,
    w_key,
    w_value,
    w_mix_out,
    expert_in,
    norm_gain,
    routes,
    route_scores,
    w_gate,
    w_up,
    w_down,
):
    mixed = mixer(
        q_latent, kv_latent, rope_key, q_gain, kv_gain, w_query, w_key, w_value, w_mix_out
    )
    expert_out = experts(expert_in, norm_gain, routes, route_scores, w_gate, w_up, w_down)
    return (mixed, expert_out)


def solution(mesh):
    in_specs = (
        P("ep", None),
        P("ep", None),
        P("ep", None),
        P(),
        P(),
        P(None, "tp"),
        P(None, "tp"),
        P(None, "tp"),
        P("tp", None),
        P("ep", None),
        P(),
        P("ep", None),
        P("ep", None),
        P("ep", None, "tp"),
        P("ep", None, "tp"),
        P("ep", "tp", None),
    )
    out_specs = (P(("ep", "tp"), None), P("ep", "tp"))
    return jax.shard_map(body, mesh=mesh, in_specs=in_specs, out_specs=out_specs, check_vma=False)
```

profile of v0, /device:TPU:0, one launch (start us, length us, event | category | flops | bytes accessed | tf_op | source)
XLA Modules:
  0.0 162.9 jit_solution(18064462734204936463)
XLA Ops:
  7.2 0.9 copy.51
  10.3 1.4 scatter_custom_fusion
  11.7 1.2 convert_reduce_fusion
  12.9 1.3 fusion.37
  14.3 1.4 fusion.39
  15.7 3.3 %gather_fusion = bf16[512,2048]{1,0:T(8,128)(2,1)} fusion(bf16[129,2048]{1,0:T(8,128)(2,1)S(1)} %concatenate.13, s32[1024]{0:T(1024)S(1)} %pad_clamp_fusion.1), kind=kCustom, calls=%fused_computation | custom fusion | bytes 4196352 | tf_op jit(solution)/shard_map/gather | solution.py:102
  19.1 6.5 %all-to-all-start = ((bf16[8,64,2048]{2,1,0:T(8,128)(2,1)}), bf16[8,64,2048]{2,1,0:T(8,128)(2,1)}, u32[]{:S(2)}, u32[]{:S(2)}) async-start(bf16[8,64,2048]{2,1,0:T(8,128)(2,1)} %bitcast.82), calls=%async_computation.1 | async-start | bytes 4194304 | tf_op jit(solution)/shard_map/all_to_all | solution.py:106
  26.1 1.5 convolution_convert_fusion.3
  27.6 47.2 %all-to-all-done = bf16[8,64,2048]{2,1,0:T(8,128)(2,1)} async-done(((bf16[8,64,2048]{2,1,0:T(8,128)(2,1)}), bf16[8,64,2048]{2,1,0:T(8,128)(2,1)}, u32[]{:S(2)}, u32[]{:S(2)}) %all-to-all-start) | async-done | bytes 2097184 | tf_op jit(solution)/shard_map/all_to_all | solution.py:106
  74.7 6.5 %fusion.5 = f32[512,1024]{1,0:T(8,128)} fusion(bf16[512,2048]{1,0:T(8,128)(2,1)} %bitcast.12, bf16[1,2048,1024]{2,1,0:T(8,128)(2,1)} %param.29), kind=kOutput, calls=%fused_computation.10 | convolution fusion | flops 2147483648 | bytes 8388608 | tf_op jit(solution)/shard_map/dot_general | solution.py:109
  81.2 10.6 %fusion.12 = bf16[2048,512]{0,1:T(8,128)(2,1)} fusion(bf16[1,1024,2048]{2,1,0:T(8,128)(2,1)} %param.31, f32[512,1024]{1,0:T(8,128)} %fusion.5, bf16[512,2048]{1,0:T(8,128)(2,1)} %bitcast.12, bf16[1,2048,1024]{2,1,0:T(8,128)(2,1)} %param.30), kind=kOutput, calls=%fused_computation.17 | convolution fusion | flops 4299161600 | bytes 14680064 | tf_op jit(solution)/shard_map/dot_general | solution.py:113
  92.5 14.2 %all-gather = bf16[8,192,64]{1,2,0:T(8,128)(2,1)S(1)} all-gather(bf16[1,192,64]{1,2,0:T(8,128)(2,1)S(1)} %maximum_bitcast_fusion), channel_id=1, replica_groups=mesh['ep'=8,'tp'=4] {'ep'}, dimensions={0}, use_global_device_ids=true | all-gather | bytes 221184 | tf_op jit(solution)/shard_map/all_gather | solution.py:51
  107.4 16.3 %all_gather.6 = bf16[1536,256]{1,0:T(8,128)(2,1)S(1)} all-gather(bf16[192,256]{1,0:T(8,128)(2,1)S(1)} %fusion.47), channel_id=1, replica_groups=mesh['ep'=8,'tp'=4] {'ep'}, dimensions={0}, use_global_device_ids=true | all-gather | bytes 884736 | tf_op jit(solution)/shard_map/all_gather | solution.py:50
  123.7 1.6 convolution_convert_fusion.1
  125.3 0.8 fusion.54
  126.2 0.9 fusion.65
  127.1 0.8 fusion.7
  128.7 0.9 fusion.34
  129.6 1.5 convolution_convert_fusion.2
  131.2 3.5 %all-to-all-start.1 = ((bf16[512,8,64]{0,2,1:T(8,128)(2,1)}), bf16[512,8,64]{0,2,1:T(8,128)(2,1)S(1)}, u32[]{:S(2)}, u32[]{:S(2)}) async-start(bf16[512,8,64]{0,2,1:T(8,128)(2,1)} %bitcast.86), calls=%async_computation.3 | async-start | bytes 1048576 | tf_op jit(solution)/shard_map/all_to_all | solution.py:121
  135.2 14.7 %all-to-all-done.1 = bf16[512,8,64]{0,2,1:T(8,128)(2,1)S(1)} async-done(((bf16[512,8,64]{0,2,1:T(8,128)(2,1)}), bf16[512,8,64]{0,2,1:T(8,128)(2,1)S(1)}, u32[]{:S(2)}, u32[]{:S(2)}) %all-to-all-start.1) | async-done | bytes 524320 | tf_op jit(solution)/shard_map/all_to_all | solution.py:121
  149.9 1.2 gather_fusion.1
  151.2 1.5 multiply_reduce_fusion
  152.7 3.4 %reduce-scatter.3.cloned.1.call-done = bf16[48,2048]{1,0:T(8,128)(2,1)} async-done(((bf16[192,2048]{1,0:T(8,128)(2,1)}), bf16[48,2048]{1,0:T(8,128)(2,1)}) %reduce-scatter.3.cloned.1.call-update) | async-done | bytes 196624 | tf_op jit(solution)/shard_map/reduce_scatter | solution.py:72
  (74 shorter events, 5.5 us)
Async XLA Ops:
  7.2 122.4 %copy-start = (bf16[512,2048]{1,0:T(8,128)(2,1)S(1)}, bf16[512,2048]{1,0:T(8,128)(2,1)}, u32[]{:S(2)}) copy-start(bf16[512,2048]{1,0:T(8,128)(2,1)} %param.24) | copy-start | bytes 6291460
  19.1 6.5 %copy-start.5 = (bf16[192,64]{0,1:T(8,128)(2,1)S(1)}, bf16[192,64]{0,1:T(8,128)(2,1)}, u32[]{:S(2)}) copy-start(bf16[192,64]{0,1:T(8,128)(2,1)} %param.18) | copy-start | bytes 73732
  19.1 6.6 %copy-start.2 = (bf16[192,512]{1,0:T(8,128)(2,1)S(1)}, bf16[192,512]{1,0:T(8,128)(2,1)}, u32[]{:S(2)}) copy-start(bf16[192,512]{1,0:T(8,128)(2,1)} %param.16) | copy-start | bytes 589828
  19.1 7.0 %copy-start.8 = (f32[512]{0:T(512)S(1)}, f32[512]{0:T(512)}, u32[]{:S(2)}) copy-start(f32[512]{0:T(512)} %param.19) | copy-start | bytes 6148
  19.1 55.6 %all-to-all-start = ((bf16[8,64,2048]{2,1,0:T(8,128)(2,1)}), bf16[8,64,2048]{2,1,0:T(8,128)(2,1)}, u32[]{:S(2)}, u32[]{:S(2)}) async-start(bf16[8,64,2048]{2,1,0:T(8,128)(2,1)} %bitcast.82), calls=%async_computation.1 | async-start | bytes 4194304 | tf_op jit(solution)/shard_map/all_to_all | solution.py:106
  25.6 105.6 %reduce-scatter.5.cloned.1.call-start = ((), (), s32[]{:S(2)}) async-start(), calls=%async_computation.5 | async-start | bytes 2621440 | tf_op jit(solution)/shard_map/reduce_scatter | solution.py:112
  91.8 15.3 %copy-start.3 = (bf16[192,256]{1,0:T(8,128)(2,1)S(1)}, bf16[192,256]{1,0:T(8,128)(2,1)}, u32[]{:S(2)}) copy-start(bf16[192,256]{1,0:T(8,128)(2,1)} %param.17) | copy-start | bytes 294916
  91.8 15.5 %copy-start.9 = (f32[256]{0:T(256)S(1)}, f32[256]{0:T(256)}, u32[]{:S(2)}) copy-start(f32[256]{0:T(256)} %param.20) | copy-start | bytes 3076
  91.8 64.3 %reduce-scatter.3.cloned.1.call-start = ((), (), s32[]{:S(2)}) async-start(), calls=%async_computation.4 | async-start | bytes 983040 | tf_op jit(solution)/shard_map/reduce_scatter | solution.py:72
  92.3 31.4 %copy-start.1 = (bf16[192,4,192]{2,1,0:T(4,128)(2,1)}, bf16[192,4,192]{2,1,0:T(4,128)(2,1)S(1)}, u32[]{:S(2)}) copy-start(bf16[192,4,192]{2,1,0:T(4,128)(2,1)S(1)} %reshape.186) | copy-start | bytes 884740
  125.3 0.9 slice-start
  127.1 1.0 copy-start.4
  129.6 5.3 %copy-start.6 = (s32[128,2]{0,1:T(2,128)S(1)}, s32[128,2]{0,1:T(2,128)}, u32[]{:S(2)}) copy-start(s32[128,2]{0,1:T(2,128)} %param.27) | copy-start | bytes 3076
  129.6 5.5 %copy-start.7 = (f32[128,2]{0,1:T(2,128)S(1)}, f32[128,2]{0,1:T(2,128)}, u32[]{:S(2)}) copy-start(f32[128,2]{0,1:T(2,128)} %param.28) | copy-start | bytes 3076
  131.2 18.8 %all-to-all-start.1 = ((bf16[512,8,64]{0,2,1:T(8,128)(2,1)}), bf16[512,8,64]{0,2,1:T(8,128)(2,1)S(1)}, u32[]{:S(2)}, u32[]{:S(2)}) async-start(bf16[512,8,64]{0,2,1:T(8,128)(2,1)} %bitcast.86), calls=%async_computation.3 | async-start | bytes 1048576 | tf_op jit(solution)/shard_map/all_to_all | solution.py:121
Sparse Core Ops, SparseCore 0:
  91.9 34.1 reduce-scatter.4
  131.3 24.7 reduce-scatter.2
where the time goes:
time: 164 us; the launch traced here: 163 us
  waiting for transfers between devices  65.3 us (40%)
  blocking collectives  30.5 us (19%)
  matrix products  24.9 us (15%)
  between operations  14.4 us (9%)
  starting transfers between devices  10.1 us (6%)
  local copies, waits for them, and re-layouts  9.44 us (6%)
  other arithmetic  8.38 us (5%)
    all_to_all x1, waiting for transfers between devices, experts(): lax.all_to_all(outgoing, 'ep', split_axis=0, concat_axis=0, tiled=True)  47.2 us
    all_gather x1, blocking collectives, mixer(): latent = lax.all_gather(kv_normed, 'ep', axis=0, tiled=True)  16.3 us
    all_to_all x1, waiting for transfers between devices, experts(): lax.all_to_all(summed.reshape(feature_count, expert_count, slots), 'ep',...  14.7 us
    all_gather x1, blocking collectives, mixer(): turned = lax.all_gather(key_turned, 'ep', axis=0, tiled=True)  14.2 us
    dot_general x1, matrix products, experts(): lax.dot_general(down_weight, hidden, (((0,), (1,)), ((), ())), preferred_...  10.6 us
    all_to_all x1, starting transfers between devices, experts(): lax.all_to_all(outgoing, 'ep', split_axis=0, concat_axis=0, tiled=True)  6.49 us
    dot_general x1, matrix products, experts(): gate = jnp.dot(arrived, gate_weight, preferred_element_type=jnp.float32)  6.48 us
    all_to_all x1, starting transfers between devices, experts(): lax.all_to_all(summed.reshape(feature_count, expert_count, slots), 'ep',...  3.5 us
  transfers between devices with their start and end apart: 4, of which 3 were waited for; matrix products, arithmetic and copies ran while one was open for 8% of the time, Pallas kernels for 0%

commit v1 on v0

v1 whole, which is shorter than its diff:
```python
import functools

import jax
import jax.numpy as jnp
from jax import lax
from jax.experimental import pallas as pl
from jax.experimental.pallas import tpu as pltpu
from jax.sharding import PartitionSpec as P

NOPE = 128
ROPE = 64
VDIM = 128


eps_norm = 1e-05
rope_base = 10000.0


MESH = pl.DeviceIdType.MESH


def remote(src, dst, send, recv, ep, tp):
    return pltpu.make_async_remote_copy(
        src_ref=src, dst_ref=dst, send_sem=send, recv_sem=recv, device_id=(ep, tp), device_id_type=MESH
    )


def greet(ep_size, tp_size, me, part):
    barrier = pltpu.get_barrier_semaphore()
    for d in range(1, ep_size):
        pl.semaphore_signal(
            barrier, inc=1, device_id=(lax.rem(me + d, ep_size), part), device_id_type=MESH
        )
    for k in range(1, tp_size):
        pl.semaphore_signal(
            barrier, inc=1, device_id=(me, lax.rem(part + k, tp_size)), device_id_type=MESH
        )
    pl.semaphore_wait(barrier, ep_size + tp_size - 2)


def gather_kernel(
    ep_size, tp_size, kv, tok, tab, okv, otok, otab,
    z_send, z_recv, t_send, t_recv, c_send, c_recv, o_send, o_recv, b_send, b_recv, local,
):
    me = lax.axis_index("ep")
    part = lax.axis_index("tp")
    levels = ep_size // 2
    level, core = me // 2, me % 2
    twin = level * 2 + 1 - core
    greet(ep_size, tp_size, me, part)
    pairs = ((kv, okv), (tok, otok))
    waits = []
    own = [pltpu.make_async_copy(tab.at[me], otab.at[me], local.at[2])]
    for a, (src, dst) in enumerate(pairs):
        own.append(pltpu.make_async_copy(src, dst.at[me], local.at[a]))
    for copy in own:
        copy.start()
    order = [d for d in range(1, levels)]
    for a, (src, dst) in enumerate(pairs):
        for d in order:
            target = lax.rem(level + d, levels) * 2 + core
            copy = remote(
                src.at[part], dst.at[me, part], z_send.at[a, d], z_recv.at[a, d], target, part
            )
            copy.start()
            waits.append(copy)
        if a == 0:
            for d in range(1, ep_size):
                target = lax.rem(me + d, ep_size)
                copy = remote(
                    tab.at[target], otab.at[me], b_send.at[d], b_recv.at[d], target, part
                )
                copy.start()
                waits.append(copy)
    for a, (src, dst) in enumerate(pairs):
        copy = remote(src, dst.at[me], o_send.at[a], o_recv.at[a], twin, part)
        copy.start()
        waits.append(copy)
    for a, (src, dst) in enumerate(pairs):
        for d in order:
            block = lax.rem(level - d + levels, levels) * 2 + core
            here = dst.at[block, part]
            remote(here, here, z_send.at[a, d], z_recv.at[a, d], twin, part).wait_recv()
            for k in range(1, tp_size):
                copy = remote(
                    here, here, t_send.at[a, d, k], t_recv.at[a, d, k],
                    me, lax.rem(part + k, tp_size),
                )
                copy.start()
                waits.append(copy)
            copy = remote(here, here, c_send.at[a, d, 0], c_recv.at[a, d, 0], twin, part)
            copy.start()
            waits.append(copy)
    for a, (src, dst) in enumerate(pairs):
        for d in order:
            block = lax.rem(level - d + levels, levels) * 2 + core
            for k in range(1, tp_size):
                here = dst.at[block, lax.rem(part - k + tp_size, tp_size)]
                remote(here, here, t_send.at[a, d, k], t_recv.at[a, d, k], twin, part).wait_recv()
                copy = remote(here, here, c_send.at[a, d, k], c_recv.at[a, d, k], twin, part)
                copy.start()
                waits.append(copy)
    for a, (src, dst) in enumerate(pairs):
        remote(src, dst.at[twin], o_send.at[a], o_recv.at[a], twin, part).wait_recv()
        for d in order:
            block = lax.rem(level - d + levels, levels) * 2 + 1 - core
            for k in range(tp_size):
                here = dst.at[block, lax.rem(part - k + tp_size, tp_size)]
                remote(here, here, c_send.at[a, d, k], c_recv.at[a, d, k], twin, part).wait_recv()
    for d in range(1, ep_size):
        source = lax.rem(me - d + ep_size, ep_size)
        here = otab.at[source]
        remote(here, here, b_send.at[d], b_recv.at[d], twin, part).wait_recv()
    for copy in waits:
        copy.wait_send()
    for copy in own:
        copy.wait()


def vmem(count):
    return [pl.BlockSpec(memory_space=pltpu.VMEM)] * count


def gather_all(kv, tok, tab):
    ep_size, tp_size = lax.axis_size("ep"), lax.axis_size("tp")
    levels = ep_size // 2
    dma = pltpu.SemaphoreType.DMA
    return pl.pallas_call(
        functools.partial(gather_kernel, ep_size, tp_size),
        out_shape=(
            jax.ShapeDtypeStruct((ep_size,) + kv.shape, kv.dtype),
            jax.ShapeDtypeStruct((ep_size,) + tok.shape, tok.dtype),
            jax.ShapeDtypeStruct(tab.shape, tab.dtype),
        ),
        in_specs=vmem(3),
        out_specs=tuple(vmem(3)),
        scratch_shapes=[
            dma((2, levels)), dma((2, levels)),
            dma((2, levels, tp_size)), dma((2, levels, tp_size)),
            dma((2, levels, tp_size)), dma((2, levels, tp_size)),
            dma((2,)), dma((2,)), dma((ep_size,)), dma((ep_size,)), dma((3,)),
        ],
        compiler_params=pltpu.CompilerParams(
            collective_id=0, has_side_effects=True, vmem_limit_bytes=60 * 1024 * 1024
        ),
    )(kv, tok, tab)


def reduce_kernel(
    ep_size, tp_size, part_ref, mix, comb, mixed, landed, mix_landed, reduced,
    p_send, p_recv, m_send, m_recv, r_send, r_recv, local,
):
    me = lax.axis_index("ep")
    part = lax.axis_index("tp")
    greet(ep_size, tp_size, me, part)
    features = comb.shape[2]
    waits = []

    def columns(index):
        return pl.ds(pl.multiple_of(index * features, features), features)

    order = [(j + ep_size // 2) % ep_size for j in range(ep_size)]
    order = [j for j in order if j != 0] + [0]
    for j in order:
        block = lax.rem(me + j, ep_size)
        for k in range(1, tp_size):
            target = lax.rem(part + k, tp_size)
            copy = remote(
                part_ref.at[block, :, columns(target)], landed.at[k, block],
                p_send.at[j, k], p_recv.at[j, k], me, target,
            )
            copy.start()
            waits.append(copy)
    for k in range(1, tp_size):
        target = lax.rem(part + k, tp_size)
        copy = remote(mix.at[target], mix_landed.at[k], m_send.at[k], m_recv.at[k], me, target)
        copy.start()
        waits.append(copy)
    for j in order:
        block = lax.rem(me + j, ep_size)
        total = part_ref[block, :, columns(part)].astype(jnp.float32)
        for k in range(1, tp_size):
            here = landed.at[k, block]
            remote(here, here, p_send.at[j, k], p_recv.at[j, k], me, part).wait_recv()
            total = total + landed[k, block].astype(jnp.float32)
        if j == 0:
            comb[me] = total.astype(jnp.bfloat16)
        else:
            reduced[block] = total.astype(jnp.bfloat16)
            copy = remote(
                reduced.at[block], comb.at[me], r_send.at[j], r_recv.at[j], block, part
            )
            copy.start()
            waits.append(copy)
    total = mix[part].astype(jnp.float32)
    for k in range(1, tp_size):
        here = mix_landed.at[k]
        remote(here, here, m_send.at[k], m_recv.at[k], me, part).wait_recv()
        total = total + mix_landed[k].astype(jnp.float32)
    mixed[...] = total.astype(jnp.bfloat16)
    for j in range(1, ep_size):
        here = comb.at[lax.rem(me - j + ep_size, ep_size)]
        remote(here, here, r_send.at[j], r_recv.at[j], me, part).wait_recv()
    for copy in waits:
        copy.wait_send()


def reduce_all(part, mix):
    ep_size, tp_size = lax.axis_size("ep"), lax.axis_size("tp")
    slots, width = part.shape[1:]
    features = width // tp_size
    dma = pltpu.SemaphoreType.DMA
    return pl.pallas_call(
        functools.partial(reduce_kernel, ep_size, tp_size),
        out_shape=(
            jax.ShapeDtypeStruct((ep_size, slots, features), jnp.bfloat16),
            jax.ShapeDtypeStruct(mix.shape[1:], jnp.bfloat16),
        ),
        in_specs=vmem(2),
        out_specs=tuple(vmem(2)),
        scratch_shapes=[
            pltpu.VMEM((tp_size, ep_size, slots, features), jnp.bfloat16),
            pltpu.VMEM(mix.shape, jnp.bfloat16),
            pltpu.VMEM((ep_size, slots, features), jnp.bfloat16),
            dma((ep_size, tp_size)), dma((ep_size, tp_size)),
            dma((tp_size,)), dma((tp_size,)), dma((ep_size,)), dma((ep_size,)), dma((1,)),
        ],
        compiler_params=pltpu.CompilerParams(
            collective_id=1, has_side_effects=True, vmem_limit_bytes=60 * 1024 * 1024
        ),
    )(part, mix)


def rms_scale(values, gain):
    wide = values.astype(jnp.float32)
    return wide * lax.rsqrt(jnp.mean(wide * wide, -1, keepdims=True) + eps_norm) * gain


def rotate(values, cosine, sine):
    first, second = jnp.split(values, 2, axis=-1)
    return jnp.concatenate([first * cosine - second * sine, first * sine + second * cosine], -1)


def angles(positions):
    inverse = rope_base ** (-jnp.arange(0, ROPE, 2).astype(jnp.float32) / ROPE)
    phase = positions[:, None] * inverse[None, :]
    return (jnp.cos(phase), jnp.sin(phase))


def latents(kv_latent, rope_key, kv_gain):
    token_count = kv_latent.shape[0]
    offset = lax.axis_index("ep") * token_count
    positions = (offset + jnp.arange(token_count, dtype=jnp.int32)).astype(jnp.float32)
    cosine, sine = angles(positions)
    kv_normed = rms_scale(kv_latent, kv_gain).astype(jnp.bfloat16)
    key_turned = rotate(rope_key.astype(jnp.float32), cosine, sine).astype(jnp.bfloat16)
    width = kv_latent.shape[1] + rope_key.shape[1]
    spare = jnp.zeros((token_count, -width % 128), jnp.bfloat16)
    return jnp.concatenate([kv_normed, key_turned, spare], 1), cosine, sine


def queries(q_latent, q_gain, w_query, cosine, sine):
    token_count = q_latent.shape[0]
    head_count = w_query.shape[1] // (NOPE + ROPE)
    q_normed = rms_scale(q_latent, q_gain).astype(jnp.bfloat16)
    query = jnp.dot(q_normed, w_query, preferred_element_type=jnp.float32).astype(jnp.bfloat16)
    query = query.reshape(token_count, head_count, NOPE + ROPE)
    q_pass = query[:, :, :NOPE]
    q_turned = rotate(
        query[:, :, NOPE:].astype(jnp.float32), cosine[:, None, :], sine[:, None, :]
    ).astype(jnp.bfloat16)
    return q_pass, q_turned


def attend(q_pass, q_turned, latent, turned, w_key, w_value, w_mix_out):
    token_count, head_count = q_pass.shape[:2]
    factor = (NOPE + ROPE) ** (-0.5)
    count = latent.shape[0]
    keys = jnp.dot(latent, w_key, preferred_element_type=jnp.float32).astype(jnp.bfloat16)
    keys = keys.reshape(count, head_count, NOPE)
    values = jnp.dot(latent, w_value, preferred_element_type=jnp.float32).astype(jnp.bfloat16)
    values = values.reshape(count, head_count, VDIM)
    scores = jnp.einsum("qhd,khd->hqk", q_pass, keys, preferred_element_type=jnp.float32)
    scores = (
        scores + jnp.einsum("qhd,kd->hqk", q_turned, turned, preferred_element_type=jnp.float32)
    ) * factor
    peak = jnp.max(scores, -1)
    weights = jnp.exp(scores - peak[:, :, None])
    total = jnp.sum(weights, -1)
    summed = jnp.einsum(
        "hqk,khd->qhd", weights.astype(jnp.bfloat16), values, preferred_element_type=jnp.float32
    )
    attended = (summed / jnp.transpose(total)[:, :, None]).astype(jnp.bfloat16)
    attended = attended.reshape(token_count, head_count * VDIM)
    return jnp.dot(attended, w_mix_out, preferred_element_type=jnp.float32).astype(jnp.bfloat16)


def routing(routes):
    token_count, choose = routes.shape
    expert_count = lax.axis_size("ep")
    slots = 2 * choose * token_count // expert_count
    flat_expert = routes.reshape(-1)
    onehot = (flat_expert[:, None] == jnp.arange(expert_count, dtype=jnp.int32)[None, :]).astype(
        jnp.int32
    )
    before = jnp.sum((jnp.cumsum(onehot, 0) - onehot) * onehot, 1)
    target = flat_expert * slots + before
    source = jnp.arange(token_count * choose, dtype=jnp.int32) // choose
    table = jnp.zeros((expert_count * slots,), jnp.int32).at[target].set(source)
    table = table.reshape(expert_count, 1, slots)
    table = jnp.pad(table, ((0, 0), (0, 7), (0, -slots % 128)))
    return target, table, slots


def normalize(expert_in, norm_gain):
    wide = expert_in.astype(jnp.float32)
    centered = wide - jnp.mean(wide, -1, keepdims=True)
    return (
        centered
        * lax.rsqrt(jnp.mean(centered * centered, -1, keepdims=True) + eps_norm)
        * norm_gain
    ).astype(jnp.bfloat16)


def body(
    q_latent,
    kv_latent,
    rope_key,
    q_gain,
    kv_gain,
    w_query,
    w_key,
    w_value,
    w_mix_out,
    expert_in,
    norm_gain,
    routes,
    route_scores,
    w_gate,
    w_up,
    w_down,
):
    ep_size, tp_size = lax.axis_size("ep"), lax.axis_size("tp")
    token_count, width = expert_in.shape
    choose = routes.shape[1]
    target, table, slots = routing(routes)
    normed = normalize(expert_in, norm_gain)
    packed, cosine, sine = latents(kv_latent, rope_key, kv_gain)
    all_packed, all_normed, arrived_table = gather_all(
        packed.reshape(tp_size, -1, packed.shape[1]), normed.reshape(tp_size, -1, width), table
    )
    rank = kv_latent.shape[1]
    all_packed = all_packed.reshape(-1, packed.shape[1])
    latent, turned = all_packed[:, :rank], all_packed[:, rank : rank + ROPE]
    q_pass, q_turned = queries(q_latent, q_gain, w_query, cosine, sine)
    mix = attend(q_pass, q_turned, latent, turned, w_key, w_value, w_mix_out)
    index = arrived_table[:, 0, :slots] + jnp.arange(ep_size, dtype=jnp.int32)[:, None] * token_count
    arrived = jnp.take(all_normed.reshape(-1, width), index.reshape(-1), axis=0, mode="clip")
    gate = jnp.dot(arrived, w_gate[0], preferred_element_type=jnp.float32)
    up = jnp.dot(arrived, w_up[0], preferred_element_type=jnp.float32)
    hidden = (jax.nn.silu(gate) * up).astype(jnp.bfloat16)
    part = jnp.dot(hidden, w_down[0], preferred_element_type=jnp.float32).astype(jnp.bfloat16)
    comb, mixed = reduce_all(
        part.reshape(ep_size, slots, width), mix.reshape(tp_size, -1, mix.shape[1])
    )
    shares = route_scores / jnp.sum(route_scores, -1, keepdims=True)
    picked = jnp.take(comb.reshape(ep_size * slots, -1), target, axis=0, mode="clip")
    picked = picked.reshape(token_count, choose, -1).astype(jnp.float32)
    expert_out = jnp.sum(picked * shares[:, :, None], 1).astype(jnp.bfloat16)
    return (mixed, expert_out)


def solution(mesh):
    in_specs = (
        P("ep", None),
        P("ep", None),
        P("ep", None),
        P(),
        P(),
        P(None, "tp"),
        P(None, "tp"),
        P(None, "tp"),
        P("tp", None),
        P("ep", None),
        P(),
        P("ep", None),
        P("ep", None),
        P("ep", None, "tp"),
        P("ep", None, "tp"),
        P("ep", "tp", None),
    )
    out_specs = (P(("ep", "tp"), None), P("ep", "tp"))
    return jax.shard_map(body, mesh=mesh, in_specs=in_specs, out_specs=out_specs, check_vma=False)
```

time: 164 us -> 139 us (0.85)
  Pallas kernels: 0 us -> 80.2 us
  waiting for transfers between devices: 65.3 us -> 0 us
  blocking collectives: 30.5 us -> 0 us
  between operations: 14.4 us -> 0.94 us
  local copies, waits for them, and re-layouts: 9.44 us -> 20.8 us
  starting transfers between devices: 10.1 us -> 0 us
  other arithmetic: 8.38 us -> 12.2 us
    pallas_call x0 -> x2, Pallas kernels: none -> 80.2 us  [the longest x1 41.6 us: reduce_all(): pl.pallas_call(functools.partial(reduce_kernel, ep_size, tp_size), out_sh...]
    all_to_all x2 -> x0, waiting for transfers between devices: 61.9 us -> none  [the longest x1 47.2 us: experts(): lax.all_to_all(outgoing, 'ep', split_axis=0, concat_axis=0, tiled=True)]
    all_gather x2 -> x0, blocking collectives: 30.5 us -> none  [the longest x1 16.3 us: mixer(): latent = lax.all_gather(kv_normed, 'ep', axis=0, tiled=True)]
    all_to_all x2 -> x0, starting transfers between devices: 10 us -> none  [the longest x1 6.49 us: experts(): lax.all_to_all(outgoing, 'ep', split_axis=0, concat_axis=0, tiled=True)]
    gather x3 -> x2, local copies, waits for them, and re-layouts: 4.6 us -> 10.4 us  [the longest x1 8 us: body(): jnp.take(all_normed.reshape(-1, width), index.reshape(-1), axis=0, mode='...]
    reduce_scatter x2 -> x0, waiting for transfers between devices: 3.39 us -> none  [the longest x1 3.37 us: mixer(): lax.psum_scatter(jnp.dot(attended, w_mix_out, preferred_element_type=jnp....]
    convert_element_type x6, other arithmetic: 1.55 us -> 4 us  [the longest x1 1.16 us: normalize(): return (centered * lax.rsqrt(jnp.mean(centered * centered, -1, keepdims=T...]
    slice x4 -> x5, local copies, waits for them, and re-layouts: 0.39 us -> 2.27 us  [the longest x1 1 us: queries(): query[:, :, NOPE:].astype(jnp.float32)]
  transfers between devices with their start and end apart: 4 -> 0, of which waited for: 3 -> 0; matrix products, arithmetic and copies ran while one was open for 8% -> 0% of each run, Pallas kernels for 0% -> 0%
where the time goes in v1:
time: 139 us
  Pallas kernels  80.2 us (58%)
  matrix products  24.7 us (18%)
  local copies, waits for them, and re-layouts  20.8 us (15%)
  other arithmetic  12.2 us (9%)
    pallas_call x1, Pallas kernels, reduce_all(): pl.pallas_call(functools.partial(reduce_kernel, ep_size, tp_size), out_sh...  41.6 us
    pallas_call x1, Pallas kernels, gather_all(): pl.pallas_call(functools.partial(gather_kernel, ep_size, tp_size), out_sh...  38.6 us
    dot_general x1, matrix products, body(): jnp.dot(hidden, w_down[0], preferred_element_type=jnp.float32)  10.7 us
    gather x1, local copies, waits for them, and re-layouts, body(): jnp.take(all_normed.reshape(-1, width), index.reshape(-1), axis=0, mode='...  8 us
    dot_general x1, matrix products, body(): gate = jnp.dot(arrived, w_gate[0], preferred_element_type=jnp.float32)  6.45 us

profile of v1, /device:TPU:0, one launch (start us, length us, event | category | flops | bytes accessed | tf_op | source)
XLA Modules:
  0.0 138.8 jit_solution(13904302099554762022)
XLA Ops:
  0.7 0.9 convert_element_type.82
  1.6 0.8 multiply_cosine_fusion
  2.7 1.0 fusion.42
  3.7 1.0 fusion.44
  5.5 1.2 convert_reduce_fusion
  6.7 1.3 fusion.31
  8.1 1.2 fusion.33
  10.9 1.4 %scatter_custom_fusion = s32[512]{0:T(512)S(1)} fusion(s32[256]{0:T(256)S(1)} %bitcast.81, s32[256]{0:T(256)S(1)} %and_select_fusion, s32[]{:T(128)} %constant.58.clone.1), kind=kCustom, calls=%fused_computation.79 | custom fusion | bytes 2052 | tf_op jit(solution)/shard_map/scatter | solution.py:309
  13.0 38.6 %shard_map.167 = (bf16[8,4,48,384]{3,2,1,0:T(8,128)(2,1)}, bf16[8,4,32,2048]{3,2,1,0:T(8,128)(2,1)}, s32[8,8,128]{2,1,0:T(8,128)}) custom-call(bf16[4,48,384]{2,1,0:T(8,128)(2,1)} %bitcast.76, bf16[4,32,2048]{2,1,0:T(8,128)(2,1)} %bitcast.74, s32[8,8,128]{2,1,0:T(8,128)} %pad.4.tab), custom_call_target="tpu_custom_call" | custom-call | tf_op jit(solution)/shard_map/pallas_call | solution.py:128
  52.6 8.0 %gather_fusion = bf16[512,2048]{1,0:T(8,128)(2,1)} fusion(bf16[1024,2048]{1,0:T(8,128)(2,1)} %bitcast.66, s32[1024]{0:T(1024)S(1)} %pad_clamp_fusion.1), kind=kCustom, calls=%fused_computation | custom fusion | bytes 4196352 | tf_op jit(solution)/shard_map/jit(_take)/gather | solution.py:358
  60.6 6.4 %fusion.5 = f32[512,1024]{1,0:T(8,128)} fusion(bf16[512,2048]{1,0:T(8,128)(2,1)} %gather_fusion, bf16[1,2048,1024]{2,1,0:T(8,128)(2,1)} %param.29), kind=kOutput, calls=%fused_computation.10 | convolution fusion | flops 2147483648 | bytes 8388608 | tf_op jit(solution)/shard_map/dot_general | solution.py:359
  67.1 10.7 %fusion.9 = bf16[512,2048]{1,0:T(8,128)(2,1)} fusion(bf16[1,1024,2048]{2,1,0:T(8,128)(2,1)} %param.31, f32[512,1024]{1,0:T(8,128)} %fusion.5, bf16[512,2048]{1,0:T(8,128)(2,1)} %gather_fusion, bf16[1,2048,1024]{2,1,0:T(8,128)(2,1)} %param.30), kind=kOutput, calls=%fused_computation.14 | convolution fusion | flops 4299161600 | bytes 14680064 | tf_op jit(solution)/shard_map/dot_general | solution.py:362
  77.8 1.8 %convolution_convert_fusion.1 = bf16[1536,512]{0,1:T(8,128)(2,1)} fusion(bf16[256,512]{1,0:T(8,128)(2,1)S(1)} %copy-done.6, bf16[1536,384]{1,0:T(8,128)(2,1)S(1)} %bitcast.70), kind=kOutput, calls=%fused_computation.16 | convolution fusion | flops 403439616 | bytes 2621440 | tf_op jit(solution)/shard_map/dot_general | solution.py:281
  79.7 1.1 convolution_convert_fusion.3
  80.8 2.1 %reshape.226 = bf16[192,4,192]{2,1,0:T(4,128)(2,1)} reshape(bf16[192,768]{1,0:T(8,128)(2,1)} %convolution_convert_fusion.3) | data formatting | bytes 589824 | tf_op jit(solution)/shard_map/reshape | solution.py:267
  82.9 1.0 slice.36
  84.7 0.9 convert_element_type.96
  85.7 0.8 fusion.41
  87.6 0.9 fusion.61
  89.9 0.9 fusion.28
  90.7 1.5 %convolution_convert_fusion.2 = bf16[192,2048]{1,0:T(8,128)(2,1)} fusion(bf16[512,2048]{1,0:T(8,128)(2,1)S(1)} %copy-done, bf16[4,24,8,128]{3,2,1,0:T(8,128)(2,1)S(1)} %fusion.28), kind=kOutput, calls=%fused_computation.17 | convolution fusion | flops 403046400 | bytes 3080192 | tf_op jit(solution)/shard_map/dot_general | solution.py:295
  92.2 41.6 %shard_map.168 = (bf16[8,64,512]{2,1,0:T(8,128)(2,1)}, bf16[48,2048]{1,0:T(8,128)(2,1)}) custom-call(bf16[8,64,2048]{2,1,0:T(8,128)(2,1)} %bitcast.75, bf16[4,48,2048]{2,1,0:T(8,128)(2,1)} %bitcast.73), custom_call_target="tpu_custom_call" | custom-call | tf_op jit(solution)/shard_map/pallas_call | solution.py:213
  133.9 2.4 %gather_fusion.1 = bf16[256,512]{1,0:T(8,128)(2,1)S(1)} fusion(bf16[512,512]{1,0:T(8,128)(2,1)} %bitcast.67, s32[1024]{0:T(1024)S(1)} %pad_clamp_fusion), kind=kCustom, calls=%fused_computation.1 | custom fusion | bytes 525312 | tf_op jit(solution)/shard_map/jit(_take)/gather | solution.py:367
  136.8 1.4 multiply_reduce_fusion
  (77 shorter events, 9.1 us)
Async XLA Ops:
  0.6 90.1 %copy-start = (bf16[512,2048]{1,0:T(8,128)(2,1)S(1)}, bf16[512,2048]{1,0:T(8,128)(2,1)}, u32[]{:S(2)}) copy-start(bf16[512,2048]{1,0:T(8,128)(2,1)} %param.24) | copy-start | bytes 6291460
  0.6 7.4 %copy-start.2 = (bf16[128,2048]{1,0:T(8,128)(2,1)S(1)}, bf16[128,2048]{1,0:T(8,128)(2,1)}, u32[]{:S(2)}) copy-start(bf16[128,2048]{1,0:T(8,128)(2,1)} %param.25) | copy-start | bytes 1572868
  0.7 7.4 %copy-start.11 = (f32[2048]{0:T(1024)S(1)}, f32[2048]{0:T(1024)}, u32[]{:S(2)}) copy-start(f32[2048]{0:T(1024)} %param.26) | copy-start | bytes 24580
  0.7 8.6 %copy-start.12 = (s32[128,2]{0,1:T(2,128)S(1)}, s32[128,2]{0,1:T(2,128)}, u32[]{:S(2)}) copy-start(s32[128,2]{0,1:T(2,128)} %param.27) | copy-start | bytes 3076
  67.1 10.7 %copy-start.3 = (bf16[8,4,48,384]{3,2,1,0:T(8,128)(2,1)S(1)}, bf16[8,4,48,384]{3,2,1,0:T(8,128)(2,1)}, u32[]{:S(2)}) copy-start(bf16[8,4,48,384]{3,2,1,0:T(8,128)(2,1)} %get-tuple-element.9) | copy-start | bytes 3538948
  67.1 10.7 %copy-start.6 = (bf16[256,512]{1,0:T(8,128)(2,1)S(1)}, bf16[256,512]{1,0:T(8,128)(2,1)}, u32[]{:S(2)}) copy-start(bf16[256,512]{1,0:T(8,128)(2,1)} %param.23) | copy-start | bytes 786436
  77.8 1.8 %copy-start.5 = (bf16[192,512]{1,0:T(8,128)(2,1)S(1)}, bf16[192,512]{1,0:T(8,128)(2,1)}, u32[]{:S(2)}) copy-start(bf16[192,512]{1,0:T(8,128)(2,1)} %param.16) | copy-start | bytes 589828
  77.8 1.9 %copy-start.4 = (bf16[512,768]{1,0:T(8,128)(2,1)S(1)}, bf16[512,768]{1,0:T(8,128)(2,1)}, u32[]{:S(2)}) copy-start(bf16[512,768]{1,0:T(8,128)(2,1)} %param.21) | copy-start | bytes 2359300
  77.8 1.9 %copy-start.14 = (f32[512]{0:T(512)S(1)}, f32[512]{0:T(512)}, u32[]{:S(2)}) copy-start(f32[512]{0:T(512)} %param.19) | copy-start | bytes 6148
  79.6 6.1 %copy-start.9 = (f32[192,32]{0,1:T(8,128)S(1)}, f32[192,32]{0,1:T(8,128)}, u32[]{:S(2)}) copy-start(f32[192,32]{0,1:T(8,128)} %get-tuple-element.18) | copy-start | bytes 73732
  79.6 6.1 %copy-start.10 = (f32[192,32]{0,1:T(8,128)S(1)}, f32[192,32]{0,1:T(8,128)}, u32[]{:S(2)}) copy-start(f32[192,32]{0,1:T(8,128)} %get-tuple-element.19) | copy-start | bytes 73732
  85.7 1.0 copy-start.7
  86.6 0.9 slice-start
  88.4 1.4 %copy-start.1 = (bf16[1536,512]{0,1:T(8,128)(2,1)S(1)}, bf16[1536,512]{0,1:T(8,128)(2,1)}, u32[]{:S(2)}) copy-start(bf16[1536,512]{0,1:T(8,128)(2,1)} %convolution_convert_fusion.1) | copy-start | bytes 4718596
  133.9 2.7 %copy-start.13 = (f32[128,2]{0,1:T(2,128)S(1)}, f32[128,2]{0,1:T(2,128)}, u32[]{:S(2)}) copy-start(f32[128,2]{0,1:T(2,128)} %param.28) | copy-start | bytes 3076
  133.9 4.3 %copy-start.8 = (bf16[48,2048]{1,0:T(8,128)(2,1)S(1)}, bf16[48,2048]{1,0:T(8,128)(2,1)}, u32[]{:S(2)}) copy-start(bf16[48,2048]{1,0:T(8,128)(2,1)} %get-tuple-element.26) | copy-start | bytes 589828
